TPU v7x, 32 devices: a whole 2x2x4 slice. The times are simulated.
32 devices in a mesh: sp: 16 (over z, y, core), tp: 2 (over x).
Axes of the slice: x: 2, y: 2, z: 4, core: 2. Of those that a mesh axis runs over, the one named last changes fastest.
Arguments:
- queries: bfloat16 [16384, 1024], P('sp', 'tp'), may hold values from -8 to 8
- keyvals: bfloat16 [16384, 8, 128], P('sp', 'tp'), may hold values from -8 to 8
- head_sink_logit: float32 [16], P('tp'), may hold values from 2 to 7
- doc_ids: int32 [16384], P('sp'), may hold values from 0 to 7, never falling along the last dimension, each value on 1 to 4096 neighbouring positions
- stream_in: bfloat16 [16384, 2048], P(('sp', 'tp')), may hold values from -6 to 6
- out_weight: bfloat16 [1024, 2048], replicated, may hold values from -1.5 to 1.5
- first_gain: float32 [2048], replicated, may hold values from 0.1 to 1.9
- up_weight: bfloat16 [2048, 8192], P('sp', 'tp'), may hold values from -0.125 to 0.125
- down_weight: bfloat16 [8192, 2048], P('tp', 'sp'), may hold values from -0.0625 to 0.0625
- second_gain: float32 [2048], replicated, may hold values from 0.1 to 1.9
Outputs:
- layer_out: bfloat16 [16384, 2048], P(('sp', 'tp'))
Inputs may be any that keep to these rules, and one draw needn't show every extreme that they name: `doc_ids`: document numbers never fall along the sequence.
All inputs are finite; a program needn't handle non-finite values.
Results may differ from a plain program's by a relative error of at most 0.013.
Values may be sent and summed in bfloat16 or wider, within the bound.
A program may use at most 128 MiB of HBM per device.

v0:
```python
import jax
import jax.numpy as jnp
from jax import lax
from jax.sharding import PartitionSpec as P

HEAD_SIZE = 64
WINDOW_REACH = 128
NEG_LARGE = -1e30
NORM_EPS = 1e-05


def padded(block, sides, width):
    for axis, dim in sides:
        count = lax.axis_size(axis)
        forward = [(i, i + 1) for i in range(count - 1)]
        backward = [(target, source) for source, target in forward]
        low = lax.ppermute(
            lax.slice_in_dim(block, block.shape[dim] - width, None, axis=dim), axis, forward
        )
        high = lax.ppermute(lax.slice_in_dim(block, 0, width, axis=dim), axis, backward)
        block = jnp.concatenate([low, block, high], axis=dim)
    return block


def layer_norm(stream, gain_row):
    centre = jnp.mean(stream, axis=-1, keepdims=True)
    shifted = stream - centre
    spread = jnp.mean(shifted * shifted, axis=-1, keepdims=True)
    return shifted * lax.rsqrt(spread + NORM_EPS) * gain_row


def attend(queries, keyvals, head_sink_logit, doc_ids):
    tok_rows = queries.shape[0]
    kv_heads = keyvals.shape[1]
    heads_per_group = queries.shape[1] // (HEAD_SIZE * kv_heads)
    block_list = tok_rows // WINDOW_REACH
    score_scale = HEAD_SIZE ** (-0.5)
    doc_marks = doc_ids.astype(jnp.bfloat16)
    rim_keys, rim_docs = (
        padded(keyvals, (("sp", 0),), WINDOW_REACH),
        padded(doc_marks, (("sp", 0),), WINDOW_REACH),
    )
    padded_rows = rim_keys.reshape(block_list + 2, WINDOW_REACH, kv_heads, 2 * HEAD_SIZE)
    banded = jnp.concatenate([padded_rows[:-2], padded_rows[1:-1], padded_rows[2:]], axis=1)
    doc_ext = rim_docs.reshape(block_list + 2, WINDOW_REACH)
    doc_band = jnp.concatenate([doc_ext[:-2], doc_ext[1:-1], doc_ext[2:]], axis=1)
    offset = lax.axis_index("sp") * tok_rows
    total_rows = tok_rows * lax.axis_size("sp")
    query_pos = offset + jnp.arange(tok_rows, dtype=jnp.int32).reshape(block_list, WINDOW_REACH, 1)
    key_pos = (
        offset
        + (
            jnp.arange(block_list, dtype=jnp.int32)[:, None] * WINDOW_REACH
            + jnp.arange(3 * WINDOW_REACH, dtype=jnp.int32)[None, :]
            - WINDOW_REACH
        )[:, None, :]
    )
    allowed = (
        (jnp.abs(query_pos - key_pos) <= WINDOW_REACH)
        & (key_pos >= 0)
        & (key_pos < total_rows)
        & (doc_marks.reshape(block_list, WINDOW_REACH, 1) == doc_band[:, None, :])
    )
    query_block_list = queries.reshape(
        block_list, WINDOW_REACH, kv_heads, heads_per_group, HEAD_SIZE
    )
    scores = (
        jnp.einsum(
            "nqhgd,nkhd->nhgqk",
            query_block_list,
            banded[..., :HEAD_SIZE],
            preferred_element_type=jnp.float32,
        )
        * score_scale
    )
    scores = jnp.where(allowed[:, None, None], scores, NEG_LARGE)
    sink_col = head_sink_logit.reshape(kv_heads, heads_per_group)[None, :, :, None, None]
    highest = jnp.maximum(jnp.max(scores, axis=-1, keepdims=True), sink_col)
    powers = jnp.exp(scores - highest)
    denominator = jnp.sum(powers, axis=-1, keepdims=True) + jnp.exp(sink_col - highest)
    weights = (powers / denominator).astype(jnp.bfloat16)
    mixed_out = jnp.einsum(
        "nhgqk,nkhd->nqhgd", weights, banded[..., HEAD_SIZE:], preferred_element_type=jnp.float32
    )
    return mixed_out.astype(jnp.bfloat16).reshape(tok_rows, kv_heads * heads_per_group * HEAD_SIZE)


def per_device(
    queries,
    keyvals,
    head_sink_logit,
    doc_ids,
    stream_in,
    out_weight,
    first_gain,
    up_weight,
    down_weight,
    second_gain,
):
    up_whole = lax.all_gather(up_weight, "sp", axis=0, tiled=True)
    down_whole = lax.all_gather(down_weight, "sp", axis=1, tiled=True)
    attended = attend(queries, keyvals, head_sink_logit, doc_ids)
    tp_count = lax.axis_size("tp")
    own_rows = attended.shape[0] // tp_count
    by_peer = attended.reshape(tp_count, own_rows, attended.shape[1])
    projected = jnp.dot(
        lax.all_to_all(by_peer, "tp", split_axis=0, concat_axis=2, tiled=True)[0],
        out_weight,
        preferred_element_type=jnp.float32,
    )[None][0]
    first_stream = layer_norm(stream_in.astype(jnp.float32) + projected, first_gain).astype(
        jnp.bfloat16
    )
    hidden = jnp.dot(
        lax.all_gather(first_stream, "tp", axis=0, tiled=True),
        up_whole,
        preferred_element_type=jnp.float32,
    )
    active = jnp.square(jnp.maximum(hidden, 0.0)).astype(jnp.bfloat16)
    mixed_out = lax.psum_scatter(
        jnp.dot(active, down_whole, preferred_element_type=jnp.float32).astype(jnp.bfloat16),
        "tp",
        scatter_dimension=0,
        tiled=True,
    ).astype(jnp.float32)
    return layer_norm(first_stream.astype(jnp.float32) + mixed_out, second_gain).astype(
        jnp.bfloat16
    )


def solution(mesh):
    return jax.shard_map(
        per_device,
        mesh=mesh,
        in_specs=(
            P("sp", "tp"),
            P("sp", "tp", None),
            P("tp"),
            P("sp"),
            P(("sp", "tp"), None),
            P(),
            P(),
            P("sp", "tp"),
            P("tp", "sp"),
            P(),
        ),
        out_specs=P(("sp", "tp"), None),
        check_vma=False,
    )
```

profile of v0, /device:TPU:0, one launch (start us, length us, event | category | flops | bytes accessed | tf_op | source)
XLA Modules:
  0.0 477.8 jit_solution(12057201046544516895)
XLA Ops:
  7.3 2.4 collective-permute-start.2
  9.7 1.3 collective-permute-start.3
  11.0 1.4 copy.26
  12.4 5.8 %collective-permute-start = (bf16[128,4,128]{2,0,1:T(8,128)(2,1)S(1)}, bf16[128,4,128]{2,0,1:T(8,128)(2,1)}, u32[]{:S(2)}, u32[]{:S(2)}) collective-permute-start(bf16[128,4,128]{2,0,1:T(8,128)(2,1)S(1)} %get-tuple-element.7), channel_id=1, source_target_pairs={{0,2},{2,4},{4,6},{6,8},{8,10},{10,12},{12,14},{14,16},{16,18},{18... | collective-permute-start | bytes 393224 | tf_op jit(solution)/shard_map/ppermute | solution.py:17
  18.2 1.3 collective-permute-start.1
  20.4 2.3 copy.32
  22.6 2.1 reshape.167
  24.8 2.3 fusion.9
  29.7 1.8 pad_maximum_fusion
  31.6 2.5 fusion.1
  34.3 3.4 fusion
  37.8 3.6 fusion.11
  42.8 17.2 %all_to_all.15 = bf16[2,512,512]{1,2,0:T(8,128)(2,1)S(1)} all-to-all(bf16[2,512,512]{1,2,0:T(8,128)(2,1)S(1)} %copy.38), channel_id=1, replica_groups=mesh['sp'=16,'tp'=2] {'tp'}, dimensions={0} | all-to-all | bytes 2097152 | tf_op jit(solution)/shard_map/all_to_all | solution.py:107
  60.0 4.2 fusion.20
  64.8 1.4 copy-done
  66.1 1.9 multiply_convert_fusion.2
  69.6 56.9 %all-gather.4.cloned.1.call-done = bf16[1024,2048]{1,0:T(8,128)(2,1)} async-done(((bf16[512,2048]{1,0:T(8,128)(2,1)}), bf16[1024,2048]{1,0:T(8,128)(2,1)}) %all-gather.4.cloned.1.call-update) | async-done | bytes 4194320 | tf_op jit(solution)/shard_map/all_gather | solution.py:115
  126.5 128.6 %all-gather.6.cloned.1.call-done = bf16[2048,4096]{1,0:T(8,128)(2,1)} async-done(((bf16[128,4096]{1,0:T(8,128)(2,1)}), bf16[2048,4096]{1,0:T(8,128)(2,1)}) %all-gather.6.cloned.1.call-update) | async-done | bytes 16777232 | tf_op jit(solution)/shard_map/all_gather | solution.py:100
  255.1 22.9 %fusion.44 = bf16[1024,4096]{1,0:T(8,128)(2,1)} fusion(bf16[2048,4096]{1,0:T(8,128)(2,1)} %all-gather.6.cloned.1.call-done, bf16[1024,2048]{1,0:T(8,128)(2,1)} %all-gather.4.cloned.1.call-done), kind=kOutput, calls=%bitcast_fusion.1.clone.1 | convolution fusion | flops 17192452096 | bytes 29360128 | tf_op jit(solution)/shard_map/dot_general | solution.py:114
  278.0 107.4 %all-gather.8.cloned.1.call-done = bf16[4096,2048]{1,0:T(8,128)(2,1)} async-done(((bf16[4096,128]{1,0:T(8,128)(2,1)}), bf16[4096,2048]{1,0:T(8,128)(2,1)}) %all-gather.8.cloned.1.call-update) | async-done | bytes 16777232 | tf_op jit(solution)/shard_map/all_gather | solution.py:101
  385.4 23.7 %convolution_convert_fusion = bf16[1024,2048]{1,0:T(8,128)(2,1)} fusion(bf16[4096,2048]{1,0:T(8,128)(2,1)} %all-gather.8.cloned.1.call-done, bf16[1024,4096]{1,0:T(8,128)(2,1)} %fusion.44), kind=kOutput, calls=%fused_computation.15 | convolution fusion | flops 17181966336 | bytes 29360128 | tf_op jit(solution)/shard_map/dot_general | solution.py:121
  409.1 52.7 %reduce-scatter.2.cloned.1.call-done = bf16[512,2048]{1,0:T(8,128)(2,1)} async-done(((bf16[1024,2048]{1,0:T(8,128)(2,1)}), bf16[512,2048]{1,0:T(8,128)(2,1)}) %reduce-scatter.2.cloned.1.call-update) | async-done | bytes 2097168 | tf_op jit(solution)/shard_map/reduce_scatter | solution.py:120
  461.8 3.9 fusion.4
  467.8 3.5 multiply_convert_fusion.1
  (58 shorter events, 10.0 us)
Async XLA Ops:
  6.5 16.1 %copy-start.7 = (bf16[1024,512]{1,0:T(8,128)(2,1)S(1)}, bf16[1024,512]{1,0:T(8,128)(2,1)}, u32[]{:S(2)}) copy-start(bf16[1024,512]{1,0:T(8,128)(2,1)} %param.10) | copy-start | bytes 3145732
  6.5 18.2 %copy-start.10 = (f32[8]{0:T(128)S(1)}, f32[8]{0:T(128)}, u32[]{:S(2)}) copy-start(f32[8]{0:T(128)} %param.12) | copy-start | bytes 100
  6.5 119.9 %all-gather.4.cloned.1.call-start = ((), (), s32[]{:S(2)}) async-start(), calls=%async_computation.2 | async-start | bytes 6291456 | tf_op jit(solution)/shard_map/all_gather | solution.py:115
  7.3 17.5 %collective-permute-start.2 = (bf16[128]{0:T(256)(128)(2,1)S(1)}, bf16[128]{0:T(256)(128)(2,1)S(1)}, u32[]{:S(2)}, u32[]{:S(2)}) collective-permute-start(bf16[128]{0:T(256)(128)(2,1)S(1)} %get-tuple-element.11), channel_id=1, source_target_pairs={{0,2},{2,4},{4,6},{6,8},{8,10},{10,12},{12,14},{14,16},{16,18},{18... | collective-permute-start | bytes 776 | tf_op jit(solution)/shard_map/ppermute | solution.py:17
  9.7 15.1 %collective-permute-start.3 = (bf16[128]{0:T(256)(128)(2,1)S(1)}, bf16[128]{0:T(256)(128)(2,1)S(1)}, u32[]{:S(2)}, u32[]{:S(2)}) collective-permute-start(bf16[128]{0:T(256)(128)(2,1)S(1)} %get-tuple-element.12), channel_id=1, source_target_pairs={{2,0},{4,2},{6,4},{8,6},{10,8},{12,10},{14,12},{16,14},{18,16},{20... | collective-permute-start | bytes 776 | tf_op jit(solution)/shard_map/ppermute | solution.py:20
  12.4 14.7 %collective-permute-start = (bf16[128,4,128]{2,0,1:T(8,128)(2,1)S(1)}, bf16[128,4,128]{2,0,1:T(8,128)(2,1)}, u32[]{:S(2)}, u32[]{:S(2)}) collective-permute-start(bf16[128,4,128]{2,0,1:T(8,128)(2,1)S(1)} %get-tuple-element.7), channel_id=1, source_target_pairs={{0,2},{2,4},{4,6},{6,8},{8,10},{10,12},{12,14},{14,16},{16,18},{18... | collective-permute-start | bytes 393224 | tf_op jit(solution)/shard_map/ppermute | solution.py:17
  18.2 8.9 %collective-permute-start.1 = (bf16[128,4,128]{2,0,1:T(8,128)(2,1)S(1)}, bf16[128,4,128]{2,0,1:T(8,128)(2,1)}, u32[]{:S(2)}, u32[]{:S(2)}) collective-permute-start(bf16[128,4,128]{2,0,1:T(8,128)(2,1)S(1)} %get-tuple-element.8), channel_id=1, source_target_pairs={{2,0},{4,2},{6,4},{8,6},{10,8},{12,10},{14,12},{16,14},{18,16},{20... | collective-permute-start | bytes 393224 | tf_op jit(solution)/shard_map/ppermute | solution.py:20
  29.7 1.9 copy-start.6
  31.6 2.5 copy-start.4
  34.3 3.6 copy-start.5
  42.6 17.4 %copy-start.3 = (bf16[1024,2048]{1,0:T(8,128)(2,1)S(1)}, bf16[1024,2048]{1,0:T(8,128)(2,1)}, u32[]{:S(2)}) copy-start(bf16[1024,2048]{1,0:T(8,128)(2,1)} %param.15) | copy-start | bytes 12582916
  64.2 1.9 copy-start
  64.2 1.9 copy-start.8
  68.1 187.0 %all-gather.6.cloned.1.call-start = ((), (), s32[]{:S(2)}) async-start(), calls=%async_computation.3 | async-start | bytes 17825792 | tf_op jit(solution)/shard_map/all_gather | solution.py:100
  68.8 316.5 %all-gather.8.cloned.1.call-start = ((), (), s32[]{:S(2)}) async-start(), calls=%async_computation.4 | async-start | bytes 17825792 | tf_op jit(solution)/shard_map/all_gather | solution.py:101
  69.6 392.2 %reduce-scatter.2.cloned.1.call-start = ((), (), s32[]{:S(2)}) async-start(), calls=%async_computation.5 | async-start | bytes 6291456 | tf_op jit(solution)/shard_map/reduce_scatter | solution.py:120
  461.8 4.0 copy-start.1
  461.8 4.7 copy-start.2
  465.7 2.0 copy-start.9
Sparse Core Ops, SparseCore 0:
  68.2 58.2 all-gather.3
  128.6 126.4 all-gather.5
  257.3 128.0 all-gather.7
  409.2 52.5 reduce-scatter.1
where the time goes:
time: 478 us
  waiting for transfers between devices  347 us (73%)
  matrix products  56.9 us (12%)
  other arithmetic  21.8 us (5%)
  blocking collectives  17.2 us (4%)
  between operations  13.4 us (3%)
  starting transfers between devices  10.9 us (2%)
  local copies, waits for them, and re-layouts  10.6 us (2%)
    all_gather x1, waiting for transfers between devices, per_device(): up_whole = lax.all_gather(up_weight, 'sp', axis=0, tiled=True)  129 us
    all_gather x1, waiting for transfers between devices, per_device(): down_whole = lax.all_gather(down_weight, 'sp', axis=1, tiled=True)  107 us
    all_gather x1, waiting for transfers between devices, per_device(): lax.all_gather(first_stream, 'tp', axis=0, tiled=True)  56.9 us
    reduce_scatter x1, waiting for transfers between devices, per_device(): lax.psum_scatter(jnp.dot(active, down_whole, preferred_element_type=jnp.f...  52.7 us
    dot_general x1, matrix products, per_device(): jnp.dot(active, down_whole, preferred_element_type=jnp.float32)  23.7 us
    dot_general x1, matrix products, per_device(): jnp.dot(lax.all_gather(first_stream, 'tp', axis=0, tiled=True), up_whole,...  22.9 us
    all_to_all x1, blocking collectives, per_device(): lax.all_to_all(by_peer, 'tp', split_axis=0, concat_axis=2, tiled=True)[0]  17.2 us
  transfers between devices with their start and end apart: 8, of which 4 were waited for; matrix products, arithmetic and copies ran while one was open for 7% of the time, Pallas kernels for 0%

commit v1 on v0

--- a/solution.py
+++ b/solution.py
@@ -2,6 +2,7 @@
 import jax.numpy as jnp
 from jax import lax
 from jax.sharding import PartitionSpec as P
+from jax.lax import axis_index, ppermute, psum
 
 HEAD_SIZE = 64
 WINDOW_REACH = 128
@@ -98,7 +99,22 @@
     second_gain,
 ):
     up_whole = lax.all_gather(up_weight, "sp", axis=0, tiled=True)
-    down_whole = lax.all_gather(down_weight, "sp", axis=1, tiled=True)
+
+    def group_the_forms(incoming_x, k_dim):
+        slots = psum(1, axis_name="sp")
+        stack_in = list(map(lambda pp: (pp, (pp + 1) % slots), range(slots)))
+
+        def work_record_in(p_next):
+            if len(p_next) == slots:
+                return p_next
+            z1 = work_record_in([ppermute(p_next[0], perm=stack_in, axis_name="sp"), *p_next])
+            return z1
+
+        r1 = jnp.concatenate(work_record_in([incoming_x]), axis=k_dim)
+        reply = jnp.roll(r1, (axis_index("sp") + 1) * incoming_x.shape[k_dim], axis=k_dim)
+        return reply
+
+    down_whole = group_the_forms(down_weight, 1)
     attended = attend(queries, keyvals, head_sink_logit, doc_ids)
     tp_count = lax.axis_size("tp")
     own_rows = attended.shape[0] // tp_count

time: 478 us -> 575 us (1.20)
  local copies, waits for them, and re-layouts: 10.6 us -> 72.1 us
  waiting for transfers between devices: 347 us -> 380 us
    ppermute x0 -> x15, waiting for transfers between devices: none -> 328 us  [work_record_in(): ppermute(p_next[0], perm=stack_in, axis_name='sp')]
    all_gather x1, waiting for transfers between devices: 129 us -> 0.01 us  [per_device(): up_whole = lax.all_gather(up_weight, 'sp', axis=0, tiled=True)]
    all_gather x1 -> x0, waiting for transfers between devices: 107 us -> none  [per_device(): down_whole = lax.all_gather(down_weight, 'sp', axis=1, tiled=True)]
    all_gather x1, waiting for transfers between devices: 56.9 us -> 0.01 us  [per_device(): lax.all_gather(first_stream, 'tp', axis=0, tiled=True)]
    unnamed x23 -> x92, local copies, waits for them, and re-layouts: 3.57 us -> 60 us
  transfers between devices with their start and end apart: 8 -> 22, of which waited for: 4 -> 16; matrix products, arithmetic and copies ran while one was open for 7% -> 10% of each run, Pallas kernels for 0% -> 0%
where the time goes in v1:
time: 575 us
  waiting for transfers between devices  380 us (66%)
  local copies, waits for them, and re-layouts  72.1 us (13%)
  matrix products  57.2 us (10%)
  other arithmetic  24.6 us (4%)
  blocking collectives  16.3 us (3%)
  between operations  13.4 us (2%)
  starting transfers between devices  11.4 us (2%)
    ppermute x15, waiting for transfers between devices, work_record_in(): ppermute(p_next[0], perm=stack_in, axis_name='sp')  328 us
    unnamed x92, local copies, waits for them, and re-layouts  60 us
    reduce_scatter x1, waiting for transfers between devices, per_device(): lax.psum_scatter(jnp.dot(active, down_whole, preferred_element_type=jnp.f...  51.1 us
    dot_general x1, matrix products, per_device(): jnp.dot(lax.all_gather(first_stream, 'tp', axis=0, tiled=True), up_whole,...  21.5 us
    dot_general x1, matrix products, per_device(): jnp.dot(active, down_whole, preferred_element_type=jnp.float32)  21.3 us
    all_to_all x1, blocking collectives, per_device(): lax.all_to_all(by_peer, 'tp', split_axis=0, concat_axis=2, tiled=True)[0]  16.3 us
  transfers between devices with their start and end apart: 22, of which 16 were waited for; matrix products, arithmetic and copies ran while one was open for 10% of the time, Pallas kernels for 0%

profile of v1, /device:TPU:0, one launch (start us, length us, event | category | flops | bytes accessed | tf_op | source)
XLA Modules:
  0.0 574.6 jit_solution(10261648843819467497)
XLA Ops:
  12.3 5.2 collective-permute-start
  21.9 5.3 reshape.167
  44.7 4.9 fusion.16
  50.9 16.3 %all_to_all.15 = bf16[2,512,512]{1,2,0:T(8,128)(2,1)S(1)} all-to-all(bf16[2,512,512]{1,2,0:T(8,128)(2,1)S(1)} %copy.38), channel_id=1, replica_groups=mesh['sp'=16,'tp'=2] {'tp'}, dimensions={0} | all-to-all | bytes 2097152 | tf_op jit(solution)/shard_map/all_to_all | solution.py:123
  67.2 5.6 fusion.26
  78.8 16.1 %collective-permute-done.4 = bf16[4096,128]{1,0:T(8,128)(2,1)S(1)} collective-permute-done((bf16[4096,128]{1,0:T(8,128)(2,1)S(1)}, bf16[4096,128]{1,0:T(8,128)(2,1)S(1)}, u32[]{:S(2)}, u32[]{:S(2)}) %collective-permute-start.4) | collective-permute-done | bytes 1048608 | tf_op jit(solution)/shard_map/ppermute | solution.py:110
  94.8 16.9 %collective-permute-done.5 = bf16[4096,128]{1,0:T(8,128)(2,1)S(1)} collective-permute-done((bf16[4096,128]{1,0:T(8,128)(2,1)S(1)}, bf16[4096,128]{1,0:T(8,128)(2,1)S(1)}, u32[]{:S(2)}, u32[]{:S(2)}) %collective-permute-start.5) | collective-permute-done | bytes 1048608 | tf_op jit(solution)/shard_map/ppermute | solution.py:110
  111.8 16.9 %collective-permute-done.6 = bf16[4096,128]{1,0:T(8,128)(2,1)S(1)} collective-permute-done((bf16[4096,128]{1,0:T(8,128)(2,1)S(1)}, bf16[4096,128]{1,0:T(8,128)(2,1)S(1)}, u32[]{:S(2)}, u32[]{:S(2)}) %collective-permute-start.6) | collective-permute-done | bytes 1048608 | tf_op jit(solution)/shard_map/ppermute | solution.py:110
  129.7 16.9 %collective-permute-done.7 = bf16[4096,128]{1,0:T(8,128)(2,1)S(1)} collective-permute-done((bf16[4096,128]{1,0:T(8,128)(2,1)S(1)}, bf16[4096,128]{1,0:T(8,128)(2,1)S(1)}, u32[]{:S(2)}, u32[]{:S(2)}) %collective-permute-start.7) | collective-permute-done | bytes 1048608 | tf_op jit(solution)/shard_map/ppermute | solution.py:110
  147.5 39.3 %collective-permute-done.8 = bf16[4096,128]{1,0:T(8,128)(2,1)S(1)} collective-permute-done((bf16[4096,128]{1,0:T(8,128)(2,1)S(1)}, bf16[4096,128]{1,0:T(8,128)(2,1)S(1)}, u32[]{:S(2)}, u32[]{:S(2)}) %collective-permute-start.8) | collective-permute-done | bytes 1048608 | tf_op jit(solution)/shard_map/ppermute | solution.py:110
  187.8 23.6 %collective-permute-done.9 = bf16[4096,128]{1,0:T(8,128)(2,1)S(1)} collective-permute-done((bf16[4096,128]{1,0:T(8,128)(2,1)S(1)}, bf16[4096,128]{1,0:T(8,128)(2,1)S(1)}, u32[]{:S(2)}, u32[]{:S(2)}) %collective-permute-start.9) | collective-permute-done | bytes 1048608 | tf_op jit(solution)/shard_map/ppermute | solution.py:110
  212.4 39.5 %collective-permute-done.10 = bf16[4096,128]{1,0:T(8,128)(2,1)S(1)} collective-permute-done((bf16[4096,128]{1,0:T(8,128)(2,1)S(1)}, bf16[4096,128]{1,0:T(8,128)(2,1)S(1)}, u32[]{:S(2)}, u32[]{:S(2)}) %collective-permute-start.10) | collective-permute-done | bytes 1048608 | tf_op jit(solution)/shard_map/ppermute | solution.py:110
  252.9 38.5 %collective-permute-done.11 = bf16[4096,128]{1,0:T(8,128)(2,1)S(1)} collective-permute-done((bf16[4096,128]{1,0:T(8,128)(2,1)S(1)}, bf16[4096,128]{1,0:T(8,128)(2,1)S(1)}, u32[]{:S(2)}, u32[]{:S(2)}) %collective-permute-start.11) | collective-permute-done | bytes 1048608 | tf_op jit(solution)/shard_map/ppermute | solution.py:110
  292.3 18.2 %collective-permute-done.12 = bf16[4096,128]{1,0:T(8,128)(2,1)S(1)} collective-permute-done((bf16[4096,128]{1,0:T(8,128)(2,1)S(1)}, bf16[4096,128]{1,0:T(8,128)(2,1)S(1)}, u32[]{:S(2)}, u32[]{:S(2)}) %collective-permute-start.12) | collective-permute-done | bytes 1048608 | tf_op jit(solution)/shard_map/ppermute | solution.py:110
  311.5 16.9 %collective-permute-done.13 = bf16[4096,128]{1,0:T(8,128)(2,1)S(1)} collective-permute-done((bf16[4096,128]{1,0:T(8,128)(2,1)S(1)}, bf16[4096,128]{1,0:T(8,128)(2,1)S(1)}, u32[]{:S(2)}, u32[]{:S(2)}) %collective-permute-start.13) | collective-permute-done | bytes 1048608 | tf_op jit(solution)/shard_map/ppermute | solution.py:110
  329.5 16.9 %collective-permute-done.14 = bf16[4096,128]{1,0:T(8,128)(2,1)S(1)} collective-permute-done((bf16[4096,128]{1,0:T(8,128)(2,1)S(1)}, bf16[4096,128]{1,0:T(8,128)(2,1)S(1)}, u32[]{:S(2)}, u32[]{:S(2)}) %collective-permute-start.14) | collective-permute-done | bytes 1048608 | tf_op jit(solution)/shard_map/ppermute | solution.py:110
  347.4 16.9 %collective-permute-done.15 = bf16[4096,128]{1,0:T(8,128)(2,1)S(1)} collective-permute-done((bf16[4096,128]{1,0:T(8,128)(2,1)S(1)}, bf16[4096,128]{1,0:T(8,128)(2,1)S(1)}, u32[]{:S(2)}, u32[]{:S(2)}) %collective-permute-start.15) | collective-permute-done | bytes 1048608 | tf_op jit(solution)/shard_map/ppermute | solution.py:110
  365.2 16.9 %collective-permute-done.16 = bf16[4096,128]{1,0:T(8,128)(2,1)S(1)} collective-permute-done((bf16[4096,128]{1,0:T(8,128)(2,1)S(1)}, bf16[4096,128]{1,0:T(8,128)(2,1)S(1)}, u32[]{:S(2)}, u32[]{:S(2)}) %collective-permute-start.16) | collective-permute-done | bytes 1048608 | tf_op jit(solution)/shard_map/ppermute | solution.py:110
  383.2 17.0 %collective-permute-done.17 = bf16[4096,128]{1,0:T(8,128)(2,1)} collective-permute-done((bf16[4096,128]{1,0:T(8,128)(2,1)S(1)}, bf16[4096,128]{1,0:T(8,128)(2,1)}, u32[]{:S(2)}, u32[]{:S(2)}) %collective-permute-start.17) | collective-permute-done | bytes 1048608 | tf_op jit(solution)/shard_map/ppermute | solution.py:110
  400.2 17.2 %collective-permute-done.18 = bf16[4096,128]{1,0:T(8,128)(2,1)} collective-permute-done((bf16[4096,128]{1,0:T(8,128)(2,1)}, bf16[4096,128]{1,0:T(8,128)(2,1)}, u32[]{:S(2)}, u32[]{:S(2)}) %collective-permute-start.18) | collective-permute-done | bytes 1048608 | tf_op jit(solution)/shard_map/ppermute | solution.py:110
  462.5 21.5 %fusion.54 = bf16[1024,4096]{1,0:T(8,128)(2,1)S(1)} fusion(bf16[2048,4096]{1,0:T(8,128)(2,1)} %all-gather.5.cloned.1.call-done, bf16[1024,2048]{1,0:T(8,128)(2,1)} %all-gather.3.cloned.1.call-done), kind=kOutput, calls=%bitcast_fusion.1.clone.2 | convolution fusion | flops 17192452096 | bytes 29360128 | tf_op jit(solution)/shard_map/dot_general | solution.py:130
  484.1 21.3 %fusion.7 = bf16[1024,2048]{1,0:T(8,128)(2,1)} fusion(bf16[4096,4096]{1,0:T(8,128)(2,1)} %constant_dynamic-update-slice_fusion, s32[]{:T(128)S(6)} %select_n.19, bf16[1024,4096]{1,0:T(8,128)(2,1)S(1)} %fusion.54), kind=kOutput, calls=%fused_computation.17 | convolution fusion | flops 17181966336 | bytes 29360132 | tf_op jit(solution)/shard_map/dot_general | solution.py:137
  505.3 51.1 %reduce-scatter.2.cloned.1.call-done = bf16[512,2048]{1,0:T(8,128)(2,1)} async-done(((bf16[1024,2048]{1,0:T(8,128)(2,1)}), bf16[512,2048]{1,0:T(8,128)(2,1)}) %reduce-scatter.2.cloned.1.call-update) | async-done | bytes 2097168 | tf_op jit(solution)/shard_map/reduce_scatter | solution.py:136
  560.4 4.1 multiply_reduce_fusion
  (155 shorter events, 98.2 us)
Async XLA Ops:
  6.5 456.0 %all-gather.3.cloned.1.call-start = ((), (), s32[]{:S(2)}) async-start(), calls=%async_computation.2 | async-start | bytes 6291456 | tf_op jit(solution)/shard_map/all_gather | solution.py:131
  7.2 20.8 %collective-permute-start.2 = (bf16[128]{0:T(256)(128)(2,1)S(1)}, bf16[128]{0:T(256)(128)(2,1)S(1)}, u32[]{:S(2)}, u32[]{:S(2)}) collective-permute-start(bf16[128]{0:T(256)(128)(2,1)S(1)} %get-tuple-element.11), channel_id=1, source_target_pairs={{0,2},{2,4},{4,6},{6,8},{8,10},{10,12},{12,14},{14,16},{16,18},{18... | collective-permute-start | bytes 776 | tf_op jit(solution)/shard_map/ppermute | solution.py:18
  9.6 18.4 %collective-permute-start.3 = (bf16[128]{0:T(256)(128)(2,1)S(1)}, bf16[128]{0:T(256)(128)(2,1)S(1)}, u32[]{:S(2)}, u32[]{:S(2)}) collective-permute-start(bf16[128]{0:T(256)(128)(2,1)S(1)} %get-tuple-element.12), channel_id=1, source_target_pairs={{2,0},{4,2},{6,4},{8,6},{10,8},{12,10},{14,12},{16,14},{18,16},{20... | collective-permute-start | bytes 776 | tf_op jit(solution)/shard_map/ppermute | solution.py:21
  12.3 18.0 %collective-permute-start = (bf16[128,4,128]{2,0,1:T(8,128)(2,1)S(1)}, bf16[128,4,128]{2,0,1:T(8,128)(2,1)S(1)}, u32[]{:S(2)}, u32[]{:S(2)}) collective-permute-start(bf16[128,4,128]{2,0,1:T(8,128)(2,1)S(1)} %get-tuple-element.7), channel_id=1, source_target_pairs={{0,2},{2,4},{4,6},{6,8},{8,10},{10,12},{12,14},{14,16},{16,18},{18... | collective-permute-start | bytes 393224 | tf_op jit(solution)/shard_map/ppermute | solution.py:18
  17.5 13.5 %collective-permute-start.1 = (bf16[128,4,128]{2,0,1:T(8,128)(2,1)S(1)}, bf16[128,4,128]{2,0,1:T(8,128)(2,1)}, u32[]{:S(2)}, u32[]{:S(2)}) collective-permute-start(bf16[128,4,128]{2,0,1:T(8,128)(2,1)S(1)} %get-tuple-element.8), channel_id=1, source_target_pairs={{2,0},{4,2},{6,4},{8,6},{10,8},{12,10},{14,12},{16,14},{18,16},{20... | collective-permute-start | bytes 393224 | tf_op jit(solution)/shard_map/ppermute | solution.py:21
  76.8 385.8 %all-gather.5.cloned.1.call-start = ((), (), s32[]{:S(2)}) async-start(), calls=%async_computation.3 | async-start | bytes 17825792 | tf_op jit(solution)/shard_map/all_gather | solution.py:101
  77.5 478.9 %reduce-scatter.2.cloned.1.call-start = ((), (), s32[]{:S(2)}) async-start(), calls=%async_computation.4 | async-start | bytes 6291456 | tf_op jit(solution)/shard_map/reduce_scatter | solution.py:136
  77.6 17.3 %collective-permute-start.4 = (bf16[4096,128]{1,0:T(8,128)(2,1)S(1)}, bf16[4096,128]{1,0:T(8,128)(2,1)S(1)}, u32[]{:S(2)}, u32[]{:S(2)}) collective-permute-start(bf16[4096,128]{1,0:T(8,128)(2,1)S(1)} %copy-done.3), channel_id=1, source_target_pairs={{0,2},{2,4},{4,6},{6,8},{8,10},{10,12},{12,14},{14,16},{16,18},{18... | collective-permute-start | bytes 3145736 | tf_op jit(solution)/shard_map/ppermute | solution.py:110
  94.8 16.9 %collective-permute-start.5 = (bf16[4096,128]{1,0:T(8,128)(2,1)S(1)}, bf16[4096,128]{1,0:T(8,128)(2,1)S(1)}, u32[]{:S(2)}, u32[]{:S(2)}) collective-permute-start(bf16[4096,128]{1,0:T(8,128)(2,1)S(1)} %collective-permute-done.4), channel_id=1, source_target_pairs={{0,2},{2,4},{4,6},{6,8},{8,10},{10,12},{12,14},{14,16},{16,18},{18... | collective-permute-start | bytes 3145736 | tf_op jit(solution)/shard_map/ppermute | solution.py:110
  111.8 16.9 %collective-permute-start.6 = (bf16[4096,128]{1,0:T(8,128)(2,1)S(1)}, bf16[4096,128]{1,0:T(8,128)(2,1)S(1)}, u32[]{:S(2)}, u32[]{:S(2)}) collective-permute-start(bf16[4096,128]{1,0:T(8,128)(2,1)S(1)} %collective-permute-done.5), channel_id=1, source_target_pairs={{0,2},{2,4},{4,6},{6,8},{8,10},{10,12},{12,14},{14,16},{16,18},{18... | collective-permute-start | bytes 3145736 | tf_op jit(solution)/shard_map/ppermute | solution.py:110
  129.7 16.9 %collective-permute-start.7 = (bf16[4096,128]{1,0:T(8,128)(2,1)S(1)}, bf16[4096,128]{1,0:T(8,128)(2,1)S(1)}, u32[]{:S(2)}, u32[]{:S(2)}) collective-permute-start(bf16[4096,128]{1,0:T(8,128)(2,1)S(1)} %collective-permute-done.6), channel_id=1, source_target_pairs={{0,2},{2,4},{4,6},{6,8},{8,10},{10,12},{12,14},{14,16},{16,18},{18... | collective-permute-start | bytes 3145736 | tf_op jit(solution)/shard_map/ppermute | solution.py:110
  147.5 39.3 %collective-permute-start.8 = (bf16[4096,128]{1,0:T(8,128)(2,1)S(1)}, bf16[4096,128]{1,0:T(8,128)(2,1)S(1)}, u32[]{:S(2)}, u32[]{:S(2)}) collective-permute-start(bf16[4096,128]{1,0:T(8,128)(2,1)S(1)} %collective-permute-done.7), channel_id=1, source_target_pairs={{0,2},{2,4},{4,6},{6,8},{8,10},{10,12},{12,14},{14,16},{16,18},{18... | collective-permute-start | bytes 3145736 | tf_op jit(solution)/shard_map/ppermute | solution.py:110
  187.8 23.6 %collective-permute-start.9 = (bf16[4096,128]{1,0:T(8,128)(2,1)S(1)}, bf16[4096,128]{1,0:T(8,128)(2,1)S(1)}, u32[]{:S(2)}, u32[]{:S(2)}) collective-permute-start(bf16[4096,128]{1,0:T(8,128)(2,1)S(1)} %collective-permute-done.8), channel_id=1, source_target_pairs={{0,2},{2,4},{4,6},{6,8},{8,10},{10,12},{12,14},{14,16},{16,18},{18... | collective-permute-start | bytes 3145736 | tf_op jit(solution)/shard_map/ppermute | solution.py:110
  212.4 39.5 %collective-permute-start.10 = (bf16[4096,128]{1,0:T(8,128)(2,1)S(1)}, bf16[4096,128]{1,0:T(8,128)(2,1)S(1)}, u32[]{:S(2)}, u32[]{:S(2)}) collective-permute-start(bf16[4096,128]{1,0:T(8,128)(2,1)S(1)} %collective-permute-done.9), channel_id=1, source_target_pairs={{0,2},{2,4},{4,6},{6,8},{8,10},{10,12},{12,14},{14,16},{16,18},{18... | collective-permute-start | bytes 3145736 | tf_op jit(solution)/shard_map/ppermute | solution.py:110
  252.9 38.5 %collective-permute-start.11 = (bf16[4096,128]{1,0:T(8,128)(2,1)S(1)}, bf16[4096,128]{1,0:T(8,128)(2,1)S(1)}, u32[]{:S(2)}, u32[]{:S(2)}) collective-permute-start(bf16[4096,128]{1,0:T(8,128)(2,1)S(1)} %collective-permute-done.10), channel_id=1, source_target_pairs={{0,2},{2,4},{4,6},{6,8},{8,10},{10,12},{12,14},{14,16},{16,18},{18... | collective-permute-start | bytes 3145736 | tf_op jit(solution)/shard_map/ppermute | solution.py:110
  292.3 18.2 %collective-permute-start.12 = (bf16[4096,128]{1,0:T(8,128)(2,1)S(1)}, bf16[4096,128]{1,0:T(8,128)(2,1)S(1)}, u32[]{:S(2)}, u32[]{:S(2)}) collective-permute-start(bf16[4096,128]{1,0:T(8,128)(2,1)S(1)} %collective-permute-done.11), channel_id=1, source_target_pairs={{0,2},{2,4},{4,6},{6,8},{8,10},{10,12},{12,14},{14,16},{16,18},{18... | collective-permute-start | bytes 3145736 | tf_op jit(solution)/shard_map/ppermute | solution.py:110
  311.5 16.9 %collective-permute-start.13 = (bf16[4096,128]{1,0:T(8,128)(2,1)S(1)}, bf16[4096,128]{1,0:T(8,128)(2,1)S(1)}, u32[]{:S(2)}, u32[]{:S(2)}) collective-permute-start(bf16[4096,128]{1,0:T(8,128)(2,1)S(1)} %collective-permute-done.12), channel_id=1, source_target_pairs={{0,2},{2,4},{4,6},{6,8},{8,10},{10,12},{12,14},{14,16},{16,18},{18... | collective-permute-start | bytes 3145736 | tf_op jit(solution)/shard_map/ppermute | solution.py:110
  329.5 16.9 %collective-permute-start.14 = (bf16[4096,128]{1,0:T(8,128)(2,1)S(1)}, bf16[4096,128]{1,0:T(8,128)(2,1)S(1)}, u32[]{:S(2)}, u32[]{:S(2)}) collective-permute-start(bf16[4096,128]{1,0:T(8,128)(2,1)S(1)} %collective-permute-done.13), channel_id=1, source_target_pairs={{0,2},{2,4},{4,6},{6,8},{8,10},{10,12},{12,14},{14,16},{16,18},{18... | collective-permute-start | bytes 3145736 | tf_op jit(solution)/shard_map/ppermute | solution.py:110
  347.4 16.9 %collective-permute-start.15 = (bf16[4096,128]{1,0:T(8,128)(2,1)S(1)}, bf16[4096,128]{1,0:T(8,128)(2,1)S(1)}, u32[]{:S(2)}, u32[]{:S(2)}) collective-permute-start(bf16[4096,128]{1,0:T(8,128)(2,1)S(1)} %collective-permute-done.14), channel_id=1, source_target_pairs={{0,2},{2,4},{4,6},{6,8},{8,10},{10,12},{12,14},{14,16},{16,18},{18... | collective-permute-start | bytes 3145736 | tf_op jit(solution)/shard_map/ppermute | solution.py:110
  365.2 16.9 %collective-permute-start.16 = (bf16[4096,128]{1,0:T(8,128)(2,1)S(1)}, bf16[4096,128]{1,0:T(8,128)(2,1)S(1)}, u32[]{:S(2)}, u32[]{:S(2)}) collective-permute-start(bf16[4096,128]{1,0:T(8,128)(2,1)S(1)} %collective-permute-done.15), channel_id=1, source_target_pairs={{0,2},{2,4},{4,6},{6,8},{8,10},{10,12},{12,14},{14,16},{16,18},{18... | collective-permute-start | bytes 3145736 | tf_op jit(solution)/shard_map/ppermute | solution.py:110
  383.2 17.0 %collective-permute-start.17 = (bf16[4096,128]{1,0:T(8,128)(2,1)S(1)}, bf16[4096,128]{1,0:T(8,128)(2,1)}, u32[]{:S(2)}, u32[]{:S(2)}) collective-permute-start(bf16[4096,128]{1,0:T(8,128)(2,1)S(1)} %collective-permute-done.16), channel_id=1, source_target_pairs={{0,2},{2,4},{4,6},{6,8},{8,10},{10,12},{12,14},{14,16},{16,18},{18... | collective-permute-start | bytes 3145736 | tf_op jit(solution)/shard_map/ppermute | solution.py:110
  400.2 17.2 %collective-permute-start.18 = (bf16[4096,128]{1,0:T(8,128)(2,1)}, bf16[4096,128]{1,0:T(8,128)(2,1)}, u32[]{:S(2)}, u32[]{:S(2)}) collective-permute-start(bf16[4096,128]{1,0:T(8,128)(2,1)} %collective-permute-done.17), channel_id=1, source_target_pairs={{0,2},{2,4},{4,6},{6,8},{8,10},{10,12},{12,14},{14,16},{16,18},{18... | collective-permute-start | bytes 3145736 | tf_op jit(solution)/shard_map/ppermute | solution.py:110
  400.2 37.7 %copy-start.5 = (bf16[4096,128]{1,0:T(8,128)(2,1)S(1)}, bf16[4096,128]{1,0:T(8,128)(2,1)}, u32[]{:S(2)}) copy-start(bf16[4096,128]{1,0:T(8,128)(2,1)} %copy-done.4) | copy-start | bytes 3145732
  505.3 59.2 %copy-start.29 = (f32[2048]{0:T(1024)S(1)}, f32[2048]{0:T(1024)}, u32[]{:S(2)}) copy-start(f32[2048]{0:T(1024)} %param.19) | copy-start | bytes 24580
  (28 other events, 333.2 us)
Sparse Core Ops, SparseCore 0:
  76.9 59.4 all-gather.2
  138.6 154.6 all-gather.4
  505.5 50.9 reduce-scatter.1
